TPU v7x, 32 devices: a whole 2x2x4 slice. The times are simulated.
32 devices in a mesh: grp: 2 (over y), sp: 4 (over z), dp: 4 (over x, core).
Axes of the slice: x: 2, y: 2, z: 4, core: 2. Of those that a mesh axis runs over, the one named last changes fastest.
Arguments:
- queries: bfloat16 [8, 512, 16, 192], P(('grp', 'dp'), 'sp'), parts along dimension 0, may hold values from -41 to 41
- kv_latent: bfloat16 [8, 512, 512], P(('grp', 'dp'), 'sp'), parts along dimension 0, may hold values from -6 to 6
- rope_key: bfloat16 [8, 512, 64], P(('grp', 'dp'), 'sp'), parts along dimension 0, may hold values from -5.1 to 5.1
- kv_gain: float32 [512], replicated, may hold values from 0.1 to 1.9
- kv_weight: bfloat16 [512, 4096], P('dp', 'sp'), may hold values from -0.25 to 0.25
- out_weight: bfloat16 [2048, 2048], P(None, 'dp'), may hold values from -1 to 1
Outputs:
- mixed: bfloat16 [8, 512, 2048], P(('grp', 'dp'), 'sp'), parts along dimension 0
There are 2 independent parts, one for each index of `grp`. A program takes and returns all parts, laid end to end along the dimension named above; an argument that names none is the same for every part. Nothing has to cross between parts.
All inputs are finite; a program needn't handle non-finite values.
Results may differ from a plain program's by a relative error of at most 0.0075.
Values may be sent and summed in bfloat16 or wider, within the bound.
A program may use at most 64 MiB of HBM per device.

v0:
```python
import jax
import jax.numpy as jnp
from jax import lax
from jax.sharding import PartitionSpec as P

NOPE = 128
VD = 128


def rotate(values, positions):
    half = values.shape[-1] // 2
    inverse = jnp.power(10000.0, -jnp.arange(half, dtype=jnp.float32) * 2.0 / values.shape[-1])
    angle = positions.astype(jnp.float32)[..., None] * inverse
    first = values[..., :half].astype(jnp.float32)
    second = values[..., half:].astype(jnp.float32)
    cosine = jnp.cos(angle)
    sine = jnp.sin(angle)
    return jnp.concatenate(
        [first * cosine - second * sine, first * sine + second * cosine], axis=-1
    )


def attend(query_rot, key_value, key_rot):
    length, heads = (query_rot.shape[0], query_rot.shape[1])
    nope = query_rot.shape[2] - key_rot.shape[1]
    scale = query_rot.shape[2] ** (-0.5)
    content = key_value[:, :, :nope]
    values = key_value[:, :, nope:]
    shared = jnp.broadcast_to(key_rot[:, None, :], (length, heads, key_rot.shape[1]))
    keys = jnp.concatenate([content, shared], axis=-1)
    block = min(512, length)
    blocks = query_rot.reshape(length // block, block, heads, query_rot.shape[2])
    key_pos = jnp.arange(length, dtype=jnp.int32)

    def one_block(item):
        query_block, index = item
        scores = (
            jnp.einsum("qhd,khd->hqk", query_block, keys, preferred_element_type=jnp.float32)
            * scale
        )
        query_pos = index * block + jnp.arange(block, dtype=jnp.int32)
        kept = query_pos[:, None] >= key_pos[None, :]
        scores = jnp.where(kept[None], scores, -jnp.inf)
        top = jnp.max(scores, axis=-1, keepdims=True)
        expo = jnp.exp(scores - top)
        probs = (expo / jnp.sum(expo, axis=-1, keepdims=True)).astype(jnp.bfloat16)
        return jnp.einsum("hqk,khd->qhd", probs, values, preferred_element_type=jnp.float32).astype(
            jnp.bfloat16
        )

    result = lax.map(one_block, (blocks, jnp.arange(length // block, dtype=jnp.int32)))
    return result.reshape(length, heads, values.shape[2])


def body(queries, kv_latent, rope_key, kv_gain, kv_weight, out_weight):
    tok_rows = queries.shape[1]
    positions = lax.axis_index("sp") * tok_rows + jnp.arange(tok_rows, dtype=jnp.int32)
    latent32 = kv_latent[0].astype(jnp.float32)
    latent_n = (
        latent32
        * lax.rsqrt(jnp.mean(latent32 * latent32, axis=-1, keepdims=True) + 1e-06)
        * kv_gain
    ).astype(jnp.bfloat16)
    key_rot = rotate(rope_key[0], positions).astype(jnp.bfloat16)
    turned = rotate(queries[0, :, :, NOPE:], positions[:, None])
    query_rot = jnp.concatenate(
        [queries[0, :, :, :NOPE].astype(jnp.float32), turned], axis=-1
    ).astype(jnp.bfloat16)
    query_heads = lax.all_to_all(query_rot[None], "sp", split_axis=2, concat_axis=1, tiled=True)
    every_latent, every_key = (
        lax.all_gather(latent_n[None], "sp", axis=1, tiled=True),
        lax.all_gather(key_rot[None], "sp", axis=1, tiled=True),
    )
    whole_latent = every_latent[0]
    kv_heads = jnp.dot(
        whole_latent,
        lax.all_gather(kv_weight, "dp", axis=0, tiled=True),
        preferred_element_type=jnp.float32,
    ).astype(jnp.bfloat16)
    kv_heads = kv_heads.reshape(whole_latent.shape[0], kv_weight.shape[1] // (NOPE + VD), NOPE + VD)
    attended = attend(query_heads[0], kv_heads, every_key[0])
    returned = lax.all_to_all(attended[None], "sp", split_axis=1, concat_axis=2, tiled=True)
    flat_rows = returned.reshape(tok_rows, returned.shape[2] * returned.shape[3])
    mixed = jnp.dot(
        flat_rows,
        lax.all_gather(out_weight, "dp", axis=1, tiled=True),
        preferred_element_type=jnp.float32,
    ).astype(jnp.bfloat16)
    return mixed[None]


def solution(mesh):
    return jax.shard_map(
        body,
        mesh=mesh,
        in_specs=(
            P(("grp", "dp"), "sp", None, None),
            P(("grp", "dp"), "sp", None),
            P(("grp", "dp"), "sp", None),
            P(),
            P("dp", "sp"),
            P(None, "dp"),
        ),
        out_specs=P(("grp", "dp"), "sp", None),
        check_vma=False,
    )
```

profile of v0, /device:TPU:0, one launch (start us, length us, event | category | flops | bytes accessed | tf_op | source)
XLA Modules:
  0.0 100.5 jit_solution(13270757476425511561)
XLA Ops:
  6.5 0.0 copy-start
  6.5 0.0 copy-start.2
  6.5 0.0 all-gather.3.cloned.1.call-start
  6.5 0.7 all-gather.3.cloned.1.call-update
  7.3 0.0 all-gather.5.cloned.1.call-start
  7.3 0.7 all-gather.5.cloned.1.call-update
  8.0 1.1 %slice.33 = bf16[1,128,16,128]{1,3,0,2:T(8,128)(2,1)S(1)} slice(bf16[1,128,16,192]{1,3,0,2:T(8,128)(2,1)} %bitcast.45), slice={[0:1], [0:128], [0:16], [0:128]} | slice | bytes 1048576 | tf_op jit(solution)/shard_map/slice | solution.py:67
  9.1 0.9 fusion.29
  10.0 1.0 slice_bitcast_fusion
  11.0 0.1 fusion.23
  11.1 0.9 pad_maximum_fusion
  12.0 6.3 %all-to-all-start = ((bf16[1,128,16,192]{1,3,0,2:T(8,128)(2,1)}), bf16[1,128,16,192]{1,3,0,2:T(8,128)(2,1)S(1)}, u32[]{:S(2)}, u32[]{:S(2)}) async-start(bf16[1,128,16,192]{1,3,0,2:T(8,128)(2,1)} %pad_maximum_fusion), calls=%async_computation | async-start | bytes 1572864 | tf_op jit(solution)/shard_map/all_to_all | solution.py:69
  18.4 25.7 %all_gather.14 = bf16[1,512,64]{1,2,0:T(8,128)(2,1)S(1)} all-gather(bf16[1,128,64]{1,2,0:T(8,128)(2,1)S(1)} %pad_maximum_fusion.1), channel_id=1, replica_groups=mesh['grp'=2,'sp'=4,'dp'=4] {'sp'}, dimensions={1}, use_global_device_ids=true | all-gather | bytes 81920 | tf_op jit(solution)/shard_map/all_gather | solution.py:72
  44.1 0.8 iota_compare_fusion
  44.9 0.0 copy-done
  44.9 0.1 fusion.15
  45.0 0.0 copy-done.2
  45.0 0.1 fusion.17
  45.1 14.7 %all_gather.12 = bf16[1,512,512]{2,1,0:T(8,128)(2,1)S(1)} all-gather(bf16[1,128,512]{2,1,0:T(8,128)(2,1)S(1)} %fusion.17), channel_id=1, replica_groups=mesh['grp'=2,'sp'=4,'dp'=4] {'sp'}, dimensions={1}, use_global_device_ids=true | all-gather | bytes 655360 | tf_op jit(solution)/shard_map/all_gather | solution.py:71
  59.8 0.0 all-to-all-done
  59.8 0.6 copy.35
  60.4 0.3 squeeze.21
  60.7 0.0 all-gather.3.cloned.1.call-done
  60.7 1.9 %convolution_convert_fusion.1 = bf16[512,1024]{1,0:T(8,128)(2,1)S(1)} fusion(bf16[512,1024]{1,0:T(8,128)(2,1)} %all-gather.3.cloned.1.call-done, bf16[1,512,512]{2,1,0:T(8,128)(2,1)S(1)} %all_gather.12), kind=kOutput, calls=%fused_computation.11 | convolution fusion | flops 537395200 | bytes 2621440 | tf_op jit(solution)/shard_map/dot_general | solution.py:75
  62.7 0.0 copy-start.1
  62.7 0.5 copy.33
  63.3 0.8 fusion.9
  64.1 0.0 copy-done.1
  64.2 2.1 %fusion.33 = (f32[4,512]{1,0:T(4,128)S(1)}, f32[4,512,512]{1,2,0:T(8,128)S(1)}) fusion(f32[4,512,512]{1,2,0:T(8,128)S(1)} %fusion.9, pred[512,512]{0,1:T(8,128)(4,1)S(1)} %copy-done.1), kind=kOutput, calls=%fused_computation.58 | output fusion | flops 6291967 | bytes 8658944 | tf_op jit(solution)/shard_map/while/body/eval_jaxpr/sub | solution.py:45
  66.3 0.5 fusion.8
  66.8 0.3 copy.29
  67.1 13.6 %all_to_all.30 = bf16[1,512,4,128]{3,2,0,1:T(4,128)(2,1)S(1)} all-to-all(bf16[1,512,4,128]{3,2,0,1:T(4,128)(2,1)S(1)} %copy.29), channel_id=1, replica_groups=mesh['grp'=2,'sp'=4,'dp'=4] {'sp'}, dimensions={1} | all-to-all | bytes 1048576 | tf_op jit(solution)/shard_map/all_to_all | solution.py:82
  80.8 0.1 copy.30
  80.8 0.3 copy.31
  81.1 7.1 %all-gather.5.cloned.1.call-done = bf16[2048,2048]{1,0:T(8,128)(2,1)} async-done(((bf16[2048,512]{1,0:T(8,128)(2,1)}), bf16[2048,2048]{1,0:T(8,128)(2,1)}) %all-gather.5.cloned.1.call-update) | async-done | bytes 8388624 | tf_op jit(solution)/shard_map/all_gather | solution.py:86
  88.2 5.5 %fusion.2 = bf16[1,128,2048]{2,1,0:T(8,128)(2,1)} fusion(bf16[128,2048]{0,1:T(8,128)(2,1)S(1)} %bitcast.39, bf16[2048,2048]{1,0:T(8,128)(2,1)} %all-gather.5.cloned.1.call-done), kind=kOutput, calls=%fused_computation.6 | convolution fusion | flops 1074003968 | bytes 9437184 | tf_op jit(solution)/shard_map/dot_general | solution.py:84
  (6 shorter events, 0.1 us)
Async XLA Ops:
  6.5 38.3 %copy-start = (bf16[1,128,512]{2,1,0:T(8,128)(2,1)S(1)}, bf16[1,128,512]{2,1,0:T(8,128)(2,1)}, u32[]{:S(2)}) copy-start(bf16[1,128,512]{2,1,0:T(8,128)(2,1)} %param.7) | copy-start | bytes 393220
  6.5 38.5 %copy-start.2 = (f32[512]{0:T(512)S(1)}, f32[512]{0:T(512)}, u32[]{:S(2)}) copy-start(f32[512]{0:T(512)} %param.9) | copy-start | bytes 6148
  6.5 54.2 %all-gather.3.cloned.1.call-start = ((), (), s32[]{:S(2)}) async-start(), calls=%async_computation.2 | async-start | bytes 1310720 | tf_op jit(solution)/shard_map/all_gather | solution.py:77
  7.3 80.9 %all-gather.5.cloned.1.call-start = ((), (), s32[]{:S(2)}) async-start(), calls=%async_computation.3 | async-start | bytes 10485760 | tf_op jit(solution)/shard_map/all_gather | solution.py:86
  12.0 47.8 %all-to-all-start = ((bf16[1,128,16,192]{1,3,0,2:T(8,128)(2,1)}), bf16[1,128,16,192]{1,3,0,2:T(8,128)(2,1)S(1)}, u32[]{:S(2)}, u32[]{:S(2)}) async-start(bf16[1,128,16,192]{1,3,0,2:T(8,128)(2,1)} %pad_maximum_fusion), calls=%async_computation | async-start | bytes 1572864 | tf_op jit(solution)/shard_map/all_to_all | solution.py:69
  62.7 1.5 %copy-start.1 = (pred[512,512]{0,1:T(8,128)(4,1)S(1)}, pred[512,512]{0,1:T(8,128)(4,1)}, u32[]{:S(2)}) copy-start(pred[512,512]{0,1:T(8,128)(4,1)} %iota_compare_fusion) | copy-start | bytes 786436
Sparse Core Ops, SparseCore 0:
  8.9 19.4 all-gather.2
  29.9 58.2 all-gather.4
where the time goes:
time: 101 us; the launch traced here: 100 us
  blocking collectives  54 us (53%)
  between operations  13.6 us (13%)
  matrix products  8.7 us (9%)
  waiting for transfers between devices  8.51 us (8%)
  starting transfers between devices  6.39 us (6%)
  other arithmetic  5.05 us (5%)
  local copies, waits for them, and re-layouts  4.24 us (4%)
    all_gather x1, blocking collectives, body(): lax.all_gather(key_rot[None], 'sp', axis=1, tiled=True)  25.7 us
    all_gather x1, blocking collectives, body(): lax.all_gather(latent_n[None], 'sp', axis=1, tiled=True)  14.7 us
    all_to_all x1, blocking collectives, body(): lax.all_to_all(attended[None], 'sp', split_axis=1, concat_axis=2, tiled=T...  13.6 us
    all_gather x1, waiting for transfers between devices, body(): lax.all_gather(out_weight, 'dp', axis=1, tiled=True)  7.08 us
    all_to_all x1, starting transfers between devices, body(): lax.all_to_all(query_rot[None], 'sp', split_axis=2, concat_axis=1, tiled=...  6.35 us
    dot_general x1, matrix products, body(): jnp.dot(flat_rows, lax.all_gather(out_weight, 'dp', axis=1, tiled=True),...  5.45 us
    sub x1, other arithmetic, one_block(): expo = jnp.exp(scores - top)  2.15 us
  transfers between devices with their start and end apart: 3, of which 1 were waited for; matrix products, arithmetic and copies ran while one was open for 12% of the time, Pallas kernels for 0%

commit v1 on v0

--- a/solution.py
+++ b/solution.py
@@ -79,7 +79,12 @@
     ).astype(jnp.bfloat16)
     kv_heads = kv_heads.reshape(whole_latent.shape[0], kv_weight.shape[1] // (NOPE + VD), NOPE + VD)
     attended = attend(query_heads[0], kv_heads, every_key[0])
-    returned = lax.all_to_all(attended[None], "sp", split_axis=1, concat_axis=2, tiled=True)
+    returned = jnp.concatenate(
+        lax.all_to_all(
+            jnp.stack(jnp.split(attended[None], lax.axis_size("sp"), axis=1)), "sp", 0, 0
+        ),
+        axis=2,
+    )
     flat_rows = returned.reshape(tok_rows, returned.shape[2] * returned.shape[3])
     mixed = jnp.dot(
         flat_rows,

time: 101 us -> 101 us (level)
  no operation moved by 1% of the time
where the time goes in v1:
time: 101 us; the launch traced here: 100 us
  blocking collectives  54 us (53%)
  between operations  13.6 us (13%)
  waiting for transfers between devices  8.96 us (9%)
  matrix products  8.7 us (9%)
  starting transfers between devices  6.39 us (6%)
  other arithmetic  5.14 us (5%)
  local copies, waits for them, and re-layouts  3.7 us (4%)
    all_gather x1, blocking collectives, body(): lax.all_gather(key_rot[None], 'sp', axis=1, tiled=True)  25.7 us
    all_gather x1, blocking collectives, body(): lax.all_gather(latent_n[None], 'sp', axis=1, tiled=True)  14.7 us
    all_to_all x1, blocking collectives, body(): lax.all_to_all(jnp.stack(jnp.split(attended[None], lax.axis_size('sp'), a...  13.6 us
    all_gather x1, waiting for transfers between devices, body(): lax.all_gather(out_weight, 'dp', axis=1, tiled=True)  7.53 us
    all_to_all x1, starting transfers between devices, body(): lax.all_to_all(query_rot[None], 'sp', split_axis=2, concat_axis=1, tiled=...  6.35 us
    dot_general x1, matrix products, body(): jnp.dot(flat_rows, lax.all_gather(out_weight, 'dp', axis=1, tiled=True),...  5.45 us
    sub x1, other arithmetic, one_block(): expo = jnp.exp(scores - top)  2.15 us
  transfers between devices with their start and end apart: 3, of which 1 were waited for; matrix products, arithmetic and copies ran while one was open for 12% of the time, Pallas kernels for 0%

profile of v1, /device:TPU:0, one launch (start us, length us, event | category | flops | bytes accessed | tf_op | source)
XLA Modules:
  0.0 100.5 jit_solution(15954829376941877631)
XLA Ops:
  6.5 0.0 copy-start
  6.5 0.0 copy-start.2
  6.5 0.0 all-gather.3.cloned.1.call-start
  6.5 0.7 all-gather.3.cloned.1.call-update
  7.3 0.0 all-gather.5.cloned.1.call-start
  7.3 0.7 all-gather.5.cloned.1.call-update
  8.0 1.1 %slice.33 = bf16[1,128,16,128]{1,3,0,2:T(8,128)(2,1)S(1)} slice(bf16[1,128,16,192]{1,3,0,2:T(8,128)(2,1)} %bitcast.51), slice={[0:1], [0:128], [0:16], [0:128]} | slice | bytes 1048576 | tf_op jit(solution)/shard_map/slice | solution.py:67
  9.1 0.9 fusion.29
  10.0 1.0 slice_bitcast_fusion
  11.0 0.1 fusion.23
  11.1 1.0 pad_maximum_fusion
  12.0 6.3 %all-to-all-start = ((bf16[1,128,16,192]{1,3,0,2:T(8,128)(2,1)}), bf16[1,128,16,192]{1,3,0,2:T(8,128)(2,1)S(1)}, u32[]{:S(2)}, u32[]{:S(2)}) async-start(bf16[1,128,16,192]{1,3,0,2:T(8,128)(2,1)} %pad_maximum_fusion), calls=%async_computation | async-start | bytes 1572864 | tf_op jit(solution)/shard_map/all_to_all | solution.py:69
  18.4 25.7 %all_gather.14 = bf16[1,512,64]{1,2,0:T(8,128)(2,1)S(1)} all-gather(bf16[1,128,64]{1,2,0:T(8,128)(2,1)S(1)} %pad_maximum_fusion.2), channel_id=1, replica_groups=mesh['grp'=2,'sp'=4,'dp'=4] {'sp'}, dimensions={1}, use_global_device_ids=true | all-gather | bytes 81920 | tf_op jit(solution)/shard_map/all_gather | solution.py:72
  44.1 0.8 iota_compare_fusion
  44.9 0.0 copy-done
  44.9 0.1 fusion.15
  45.0 0.0 copy-done.2
  45.0 0.1 fusion.17
  45.1 14.7 %all_gather.12 = bf16[1,512,512]{2,1,0:T(8,128)(2,1)S(1)} all-gather(bf16[1,128,512]{2,1,0:T(8,128)(2,1)S(1)} %fusion.17), channel_id=1, replica_groups=mesh['grp'=2,'sp'=4,'dp'=4] {'sp'}, dimensions={1}, use_global_device_ids=true | all-gather | bytes 655360 | tf_op jit(solution)/shard_map/all_gather | solution.py:71
  59.8 0.0 all-to-all-done
  59.8 0.6 copy.20
  60.4 0.3 squeeze.21
  60.7 0.0 all-gather.3.cloned.1.call-done
  60.8 1.9 %convolution_convert_fusion.1 = bf16[512,1024]{1,0:T(8,128)(2,1)S(1)} fusion(bf16[512,1024]{1,0:T(8,128)(2,1)} %all-gather.3.cloned.1.call-done, bf16[1,512,512]{2,1,0:T(8,128)(2,1)S(1)} %all_gather.12), kind=kOutput, calls=%fused_computation.11 | convolution fusion | flops 537395200 | bytes 2621440 | tf_op jit(solution)/shard_map/dot_general | solution.py:75
  62.7 0.0 copy-start.1
  62.7 0.5 copy.18
  63.3 0.8 fusion.9
  64.2 0.0 copy-done.1
  64.2 2.1 %fusion.33 = (f32[4,512]{1,0:T(4,128)S(1)}, f32[4,512,512]{1,2,0:T(8,128)S(1)}) fusion(f32[4,512,512]{1,2,0:T(8,128)S(1)} %fusion.9, pred[512,512]{0,1:T(8,128)(4,1)S(1)} %copy-done.1), kind=kOutput, calls=%fused_computation.63 | output fusion | flops 6291967 | bytes 8658944 | tf_op jit(solution)/shard_map/while/body/eval_jaxpr/sub | solution.py:45
  66.3 0.5 fusion.8
  66.8 0.1 slice_bitcast_fusion.4
  66.9 0.1 pad_maximum_fusion.1
  67.0 13.6 %all_to_all.20 = bf16[4,1,128,4,128]{2,4,3,1,0:T(8,128)(2,1)S(1)} all-to-all(bf16[4,1,128,4,128]{2,4,3,1,0:T(8,128)(2,1)S(1)} %pad_maximum_fusion.1), channel_id=1, replica_groups=mesh['grp'=2,'sp'=4,'dp'=4] {'sp'}, dimensions={0} | all-to-all | bytes 1048576 | tf_op jit(solution)/shard_map/all_to_all | solution.py:83
  80.7 7.5 %all-gather.5.cloned.1.call-done = bf16[2048,2048]{1,0:T(8,128)(2,1)} async-done(((bf16[2048,512]{1,0:T(8,128)(2,1)}), bf16[2048,2048]{1,0:T(8,128)(2,1)}) %all-gather.5.cloned.1.call-update) | async-done | bytes 8388624 | tf_op jit(solution)/shard_map/all_gather | solution.py:91
  88.2 5.5 %fusion.2 = bf16[1,128,2048]{2,1,0:T(8,128)(2,1)} fusion(bf16[128,2048]{0,1:T(8,128)(2,1)S(1)} %bitcast.46, bf16[2048,2048]{1,0:T(8,128)(2,1)} %all-gather.5.cloned.1.call-done), kind=kOutput, calls=%fused_computation.6 | convolution fusion | flops 1074003968 | bytes 9437184 | tf_op jit(solution)/shard_map/dot_general | solution.py:89
  (6 shorter events, 0.1 us)
Async XLA Ops:
  6.5 38.4 %copy-start = (bf16[1,128,512]{2,1,0:T(8,128)(2,1)S(1)}, bf16[1,128,512]{2,1,0:T(8,128)(2,1)}, u32[]{:S(2)}) copy-start(bf16[1,128,512]{2,1,0:T(8,128)(2,1)} %param.7) | copy-start | bytes 393220
  6.5 38.5 %copy-start.2 = (f32[512]{0:T(512)S(1)}, f32[512]{0:T(512)}, u32[]{:S(2)}) copy-start(f32[512]{0:T(512)} %param.9) | copy-start | bytes 6148
  6.5 54.2 %all-gather.3.cloned.1.call-start = ((), (), s32[]{:S(2)}) async-start(), calls=%async_computation.2 | async-start | bytes 1310720 | tf_op jit(solution)/shard_map/all_gather | solution.py:77
  7.3 80.9 %all-gather.5.cloned.1.call-start = ((), (), s32[]{:S(2)}) async-start(), calls=%async_computation.3 | async-start | bytes 10485760 | tf_op jit(solution)/shard_map/all_gather | solution.py:91
  12.0 47.8 %all-to-all-start = ((bf16[1,128,16,192]{1,3,0,2:T(8,128)(2,1)}), bf16[1,128,16,192]{1,3,0,2:T(8,128)(2,1)S(1)}, u32[]{:S(2)}, u32[]{:S(2)}) async-start(bf16[1,128,16,192]{1,3,0,2:T(8,128)(2,1)} %pad_maximum_fusion), calls=%async_computation | async-start | bytes 1572864 | tf_op jit(solution)/shard_map/all_to_all | solution.py:69
  62.7 1.5 %copy-start.1 = (pred[512,512]{0,1:T(8,128)(4,1)S(1)}, pred[512,512]{0,1:T(8,128)(4,1)}, u32[]{:S(2)}) copy-start(pred[512,512]{0,1:T(8,128)(4,1)} %iota_compare_fusion) | copy-start | bytes 786436
Sparse Core Ops, SparseCore 0:
  8.9 19.4 all-gather.2
  29.9 58.2 all-gather.4
